TPU v7x, 32 devices: a whole 2x2x4 slice. The times are simulated.
32 devices in a mesh: sp: 8 (over z, y), tp: 4 (over x, core).
Axes of the slice: x: 2, y: 2, z: 4, core: 2. Of those that a mesh axis runs over, the one named last changes fastest.
Arguments:
- mixer_value_projection: bfloat16 [6144, 2048], P('sp', 'tp'), may hold values from -6 to 6
- write_vectors_projected: bfloat16 [6144, 256], P('sp', 'tp'), may hold values from -6 to 6
- read_vectors_projected: bfloat16 [6144, 256], P('sp', 'tp'), may hold values from -6 to 6
- output_gate_projected: bfloat16 [6144, 2048], P('sp', 'tp'), may hold values from -6 to 6
- step_size_scores: float32 [6144, 32], P('sp', 'tp'), may hold values from -8 to 8
- position_decay_extra: float32 [6144, 32], P('sp', 'tp'), may hold values from -1 to 0
- step_size_bias: float32 [32], P('tp'), may hold values from -1 to 1
- head_decay_logarithm: float32 [32], P('tp'), may hold values from -14 to -3
- value_filter_taps: bfloat16 [4, 2048], P(None, 'tp'), may hold values from -3 to 3
- write_filter_taps: bfloat16 [4, 256], P(None, 'tp'), may hold values from -3 to 3
- read_filter_taps: bfloat16 [4, 256], P(None, 'tp'), may hold values from -3 to 3
- gated_group_norm_gain: float32 [2048], P('tp'), may hold values from 0.1 to 1.9
- mixer_output_weight: bfloat16 [2048, 2048], P('tp'), may hold values from -0.125 to 0.125
- residual: bfloat16 [6144, 2048], P('sp'), may hold values from -6 to 6
- feedforward_norm_gain: float32 [2048], replicated, may hold values from 0.1 to 1.9
- feedforward_gate_weight: bfloat16 [2048, 5632], P('sp', 'tp'), may hold values from -0.125 to 0.125
- feedforward_value_weight: bfloat16 [2048, 5632], P('sp', 'tp'), may hold values from -0.125 to 0.125
- gate_filter_taps: bfloat16 [3, 5632], P(None, 'tp'), may hold values from -3.5 to 3.5
- single_value_filter_taps: bfloat16 [3, 5632], P(None, 'tp'), may hold values from -3.5 to 3.5
- feedforward_down_weight: bfloat16 [5632, 2048], P('tp', 'sp'), may hold values from -0.078125 to 0.078125
Outputs:
- mixed: bfloat16 [6144, 2048], P(('sp', 'tp'))
All inputs are finite; a program needn't handle non-finite values.
Results may differ from a plain program's by a relative error of at most 0.012.
Values may be sent and summed in bfloat16 or wider, within the bound.
A program may use at most 192 MiB of HBM per device.

v0:
```python
import jax
import jax.numpy as jnp
from jax import lax
from jax.sharding import PartitionSpec as P

HEAD = 64
STATE = 64
BLOCK = 128
epsilon = 1e-06


def from_behind(value, axis, by):
    length = lax.axis_size(axis)
    pairs = [(i, i + by) for i in range(length) if 0 <= i + by < length]
    return lax.ppermute(value, axis, pairs)


def entering_2(value, axis, join, neutral):
    count, mine = (lax.axis_size(axis), lax.axis_index(axis))
    pieces = jax.tree.map(lambda part: lax.all_gather(part, axis), value)
    running = jax.tree.map(
        lambda part, zero: jnp.full_like(part, 0) + jnp.asarray(zero, part.dtype), value, neutral
    )

    def lap(position, running):
        longer = join(running, jax.tree.map(lambda part: part[position], pieces))
        return jax.tree.map(lambda new, old: jnp.where(position < mine, new, old), longer, running)

    return lax.fori_loop(0, count - 1, lap, running)


def causal_taps(current, previous, kernel):
    tap_count = kernel.shape[0]
    length = current.shape[0]
    padded = jnp.concatenate([previous, current], 0).astype(jnp.float32)
    result = jnp.zeros((length, current.shape[1]), jnp.float32)
    for offset in range(tap_count):
        result = result + kernel[offset].astype(jnp.float32) * padded[offset : offset + length]
    return result


def channel_norm(stream, gain):
    floats = stream.astype(jnp.float32)
    scaled = floats * lax.rsqrt(jnp.mean(floats * floats, axis=-1, keepdims=True) + epsilon)
    return (scaled * gain).astype(jnp.bfloat16)


def on_device(
    mixer_value_projection,
    write_vectors_projected,
    read_vectors_projected,
    output_gate_projected,
    step_size_scores,
    position_decay_extra,
    step_size_bias,
    head_decay_logarithm,
    value_filter_taps,
    write_filter_taps,
    read_filter_taps,
    gated_group_norm_gain,
    mixer_output_weight,
    residual,
    feedforward_norm_gain,
    feedforward_gate_weight,
    feedforward_value_weight,
    gate_filter_taps,
    single_value_filter_taps,
    feedforward_down_weight,
):
    row_count = mixer_value_projection.shape[0]
    head_count = step_size_scores.shape[1]
    group_count = write_vectors_projected.shape[1] // STATE
    per_group = head_count // group_count
    mix_rim = value_filter_taps.shape[0] - 1
    rim_values, rim_write, rim_read = from_behind(
        (
            mixer_value_projection[row_count - mix_rim :],
            write_vectors_projected[row_count - mix_rim :],
            read_vectors_projected[row_count - mix_rim :],
        ),
        "sp",
        1,
    )
    x_conv = jax.nn.silu(causal_taps(mixer_value_projection, rim_values, value_filter_taps)).astype(
        jnp.bfloat16
    )
    write_conv = jax.nn.silu(
        causal_taps(write_vectors_projected, rim_write, write_filter_taps)
    ).astype(jnp.bfloat16)
    read_conv = jax.nn.silu(causal_taps(read_vectors_projected, rim_read, read_filter_taps)).astype(
        jnp.bfloat16
    )
    step_size_head = jax.nn.softplus(step_size_scores + step_size_bias)
    logarithm_decay_rate = -step_size_head * jnp.exp(head_decay_logarithm) + position_decay_extra
    scaled = (
        x_conv.astype(jnp.float32).reshape(row_count, head_count, HEAD) * step_size_head[:, :, None]
    ).astype(jnp.bfloat16)
    block_count = row_count // BLOCK
    value_blocks = scaled.reshape(block_count, BLOCK, group_count, per_group, HEAD)
    write_blocks = write_conv.reshape(block_count, BLOCK, group_count, STATE)
    read_blocks = read_conv.reshape(block_count, BLOCK, group_count, STATE)
    running = jnp.cumsum(logarithm_decay_rate.reshape(block_count, BLOCK, head_count), axis=1)
    by_head = jnp.moveaxis(running, 1, 2)
    spread = by_head[..., :, None] - by_head[..., None, :]
    causal = jnp.tril(jnp.ones((BLOCK, BLOCK), dtype=jnp.bool_))
    decays = jnp.exp(jnp.where(causal, spread, -jnp.inf)).reshape(
        block_count, group_count, per_group, BLOCK, BLOCK
    )
    scores = jnp.einsum(
        "blgn,bsgn->bgls", read_blocks, write_blocks, preferred_element_type=jnp.float32
    )
    weights = (scores[:, :, None] * decays).astype(jnp.bfloat16)
    inside = jnp.einsum(
        "bgrls,bsgrp->blgrp", weights, value_blocks, preferred_element_type=jnp.float32
    )
    tails = jnp.moveaxis(jnp.exp(by_head[..., -1:] - by_head), 2, 1).reshape(
        block_count, BLOCK, group_count, per_group
    )
    tailed = (value_blocks.astype(jnp.float32) * tails[..., None]).astype(jnp.bfloat16)
    fresh = jnp.einsum(
        "bsgn,bsgrp->bgrnp", write_blocks, tailed, preferred_element_type=jnp.float32
    )
    block_logs = by_head[..., -1].reshape(block_count, group_count, per_group)

    def carry_step(carried, inputs):
        piece, block_log = inputs
        return (carried * jnp.exp(block_log)[..., None, None] + piece, carried)

    empty_state = jnp.zeros((group_count, per_group, STATE, HEAD), jnp.float32)
    local_end, local_before = lax.scan(carry_step, empty_state, (fresh, block_logs))
    device_log = jnp.sum(block_logs, axis=0)

    def combine(earlier, later):
        return (earlier[0] * later[0], earlier[1] * later[0][..., None, None] + later[1])

    identity = (jnp.ones((group_count, per_group), jnp.float32), empty_state)
    incoming = entering_2((jnp.exp(device_log), local_end), "sp", combine, identity)[1]
    before_block = jnp.cumsum(block_logs, axis=0) - block_logs
    entering_state = local_before + incoming[None] * jnp.exp(before_block)[..., None, None]
    entering = jnp.einsum(
        "blgn,bgrnp->blgrp",
        read_blocks.astype(jnp.float32),
        entering_state,
        precision=lax.Precision.HIGHEST,
    )
    entering = (
        entering * jnp.exp(running).reshape(block_count, BLOCK, group_count, per_group)[..., None]
    )
    mixer = (inside + entering).reshape(row_count, head_count * HEAD)
    gated = (mixer * jax.nn.silu(output_gate_projected.astype(jnp.float32))).reshape(
        row_count, group_count, -1
    )
    gated = gated * lax.rsqrt(jnp.mean(gated * gated, axis=-1, keepdims=True) + epsilon)
    normed = (gated.reshape(row_count, -1) * gated_group_norm_gain).astype(jnp.bfloat16)
    share = row_count // lax.axis_size("tp")
    tp_index = lax.axis_index("tp")
    summed = lax.psum_scatter(
        jnp.dot(normed, mixer_output_weight, preferred_element_type=jnp.float32),
        "tp",
        scatter_dimension=0,
        tiled=True,
    )
    own_residual = lax.dynamic_slice_in_dim(residual, tp_index * share, share, 0)
    stream = (own_residual.astype(jnp.float32) + summed).astype(jnp.bfloat16)
    ffn_rows = lax.all_gather(channel_norm(stream, feedforward_norm_gain), "tp", axis=0, tiled=True)
    gate_full, value_full = (
        lax.all_gather(feedforward_gate_weight, "sp", axis=0, tiled=True),
        lax.all_gather(feedforward_value_weight, "sp", axis=0, tiled=True),
    )
    gate_sum = jnp.dot(ffn_rows, gate_full, preferred_element_type=jnp.float32)
    value_sum = jnp.dot(ffn_rows, value_full, preferred_element_type=jnp.float32)
    gate_rows = gate_sum.astype(jnp.bfloat16)
    value_rows = value_sum.astype(jnp.bfloat16)
    ffn_rim = gate_filter_taps.shape[0] - 1
    rim_gate, rim_value = from_behind(
        (gate_rows[row_count - ffn_rim :], value_rows[row_count - ffn_rim :]), "sp", 1
    )
    hidden = (
        jax.nn.silu(causal_taps(gate_rows, rim_gate, gate_filter_taps))
        * causal_taps(value_rows, rim_value, single_value_filter_taps)
    ).astype(jnp.bfloat16)
    down_full = lax.all_gather(feedforward_down_weight, "sp", axis=1, tiled=True)
    partial_down = jnp.dot(hidden, down_full, preferred_element_type=jnp.float32)
    down = lax.psum_scatter(
        partial_down.astype(jnp.bfloat16), "tp", scatter_dimension=0, tiled=True
    ).astype(jnp.float32)
    return (stream.astype(jnp.float32) + down).astype(jnp.bfloat16)


def solution(mesh):
    placed = (
        P("sp", "tp"),
        P("sp", "tp"),
        P("sp", "tp"),
        P("sp", "tp"),
        P("sp", "tp"),
        P("sp", "tp"),
        P("tp"),
        P("tp"),
        P(None, "tp"),
        P(None, "tp"),
        P(None, "tp"),
        P("tp"),
        P("tp", None),
        P("sp", None),
        P(),
        P("sp", "tp"),
        P("sp", "tp"),
        P(None, "tp"),
        P(None, "tp"),
        P("tp", "sp"),
    )
    return jax.shard_map(
        on_device, mesh=mesh, in_specs=placed, out_specs=P(("sp", "tp"), None), check_vma=False
    )
```

profile of v0, /device:TPU:0, one launch (start us, length us, event | category | flops | bytes accessed | tf_op | source)
XLA Modules:
  0.0 557.1 jit_solution(11165353216714825185)
XLA Ops:
  8.2 5.7 %collective-permute-start = (bf16[3,512]{0,1:T(8,128)(2,1)}, bf16[3,512]{0,1:T(8,128)(2,1)}, u32[]{:S(2)}, u32[]{:S(2)}) collective-permute-start(bf16[3,512]{0,1:T(8,128)(2,1)} %copy.49), channel_id=1, source_target_pairs={{0,4},{4,8},{8,12},{12,16},{16,20},{20,24},{24,28},{1,5},{5,9},{9,... | collective-permute-start | bytes 9224 | tf_op jit(solution)/shard_map/ppermute | solution.py:15
  13.9 1.4 slice.146
  15.3 3.5 collective-permute-start.2
  18.8 2.3 copy.50
  21.1 1.4 slice_convert_fusion.3
  23.1 1.5 fusion.53
  25.2 1.1 slice_reduce_fusion
  30.6 1.6 maximum_convert_fusion.2
  32.2 2.7 fusion.39
  34.9 2.7 reshape.164
  37.6 2.9 multiply_convert_fusion.1
  40.5 1.5 convolution_bitcast_fusion
  42.0 15.6 %while.27 = (s32[]{:T(128)}, f32[1,8,64,64]{3,2,1,0:T(8,128)S(1)}, f32[6,1,8,64,64]{4,3,2,1,0:T(8,128)}, f32[6,1,8]{2,1,0:T(1,128)}, f32[6,1,8,64,64]{3,4,2,0,1:T(8,128)}, /*index=5*/s32[]{:T(128)}, s32[]{:T(128)}) while((s32[]{:T(128)}, f32[1,8,64,64]{3,2,1,0:T(8,128)S(1)}, f32[6,1,8,64,64]{4,3,2,1,0:T(8,128)}, ...), condition=%wide.region_2.3_spmd.clone, body=%wide.region_1.2_spmd.clone.sunk | while | flops 131075 | bytes 1311424 | solution.py:130
  59.2 2.8 collective-permute-start.1
  62.2 1.2 dynamic-slice
  64.8 19.2 %all-reduce = f32[64]{0:T(128)S(1)} all-reduce(f32[64]{0:T(128)S(1)} %exponential_dynamic-update-slice_fusion), channel_id=2, replica_groups=mesh['sp'=8,'tp'=4] {'sp'}, use_global_device_ids=true, to_apply=%add | all-reduce | flops 64 | bytes 512
  84.2 1.1 copy.66
  85.3 2.3 copy.68
  88.2 1.6 fusion.46
  89.7 17.8 %all-gather.16.cloned.1.call-done = f32[8,8,64,64]{3,2,1,0:T(8,128)} async-done(((f32[1,8,64,64]{3,2,1,0:T(8,128)}), f32[8,8,64,64]{3,2,1,0:T(8,128)}) %all-gather.16.cloned.1.call-update) | async-done | bytes 1048592 | tf_op jit(solution)/shard_map/all_gather | solution.py:20
  107.5 7.6 %while.28 = (s32[]{:T(128)}, f32[1,8,64,64]{3,2,1,0:T(8,128)S(1)}, s32[]{:T(128)}, f32[8,1,8]{2,1,0:T(1,128)S(1)}, f32[8,1,8,64,64]{4,3,2,1,0:T(8,128)}, /*index=5*/s32[]{:T(128)}, s32[]{:T(128)}) while((s32[]{:T(128)}, f32[1,8,64,64]{3,2,1,0:T(8,128)S(1)}, s32[]{:T(128)}, f32[8,1,8]{2,1,0:T(1,128)S(1)}, ...), condition=%wide.region_5.6_spmd.clone, body=%wide.region_4.5_spmd.clone.sunk | while | flops 131076 | bytes 393417 | solution.py:29
  107.5 1.0 fusion.73
  108.6 1.1 fusion.73
  109.7 1.1 fusion.73
  110.8 1.1 fusion.73
  111.8 1.1 fusion.73
  112.9 1.1 fusion.73
  114.0 1.1 fusion.73
  115.1 3.0 fusion.23
  118.1 1.3 fusion.22
  121.1 4.8 fusion.32
  126.7 56.8 %reduce-scatter.3.cloned.1.call-done = f32[192,2048]{1,0:T(8,128)} async-done(((f32[768,2048]{1,0:T(8,128)}), f32[192,2048]{1,0:T(8,128)}) %reduce-scatter.3.cloned.1.call-update) | async-done | bytes 1572880 | tf_op jit(solution)/shard_map/reduce_scatter | solution.py:157
  183.5 1.9 fusion.14
  185.5 1.1 fusion.16
  188.0 90.1 %all-gather.10.cloned.1.call-done = bf16[2048,1408]{1,0:T(8,128)(2,1)} async-done(((bf16[256,1408]{1,0:T(8,128)(2,1)}), bf16[2048,1408]{1,0:T(8,128)(2,1)}) %all-gather.10.cloned.1.call-update) | async-done | bytes 5767184 | tf_op jit(solution)/shard_map/all_gather | solution.py:167
  278.0 28.1 %all-gather.8.cloned.1.call-done = bf16[768,2048]{1,0:T(8,128)(2,1)} async-done(((bf16[192,2048]{1,0:T(8,128)(2,1)}), bf16[768,2048]{1,0:T(8,128)(2,1)}) %all-gather.8.cloned.1.call-update) | async-done | bytes 3145744 | tf_op jit(solution)/shard_map/all_gather | solution.py:165
  306.2 8.3 %convolution_convert_fusion.2 = bf16[768,1408]{1,0:T(8,128)(2,1)S(1)} fusion(bf16[768,2048]{1,0:T(8,128)(2,1)} %all-gather.8.cloned.1.call-done, bf16[2048,1408]{1,0:T(8,128)(2,1)} %all-gather.10.cloned.1.call-done), kind=kOutput, calls=%fused_computation.23 | convolution fusion | flops 4430266368 | bytes 11075584 | tf_op jit(solution)/shard_map/dot_general | solution.py:170
  314.5 1.3 copy-done.4
  315.9 3.4 collective-permute-start.3
  319.3 81.4 %all-gather.12.cloned.1.call-done = bf16[2048,1408]{1,0:T(8,128)(2,1)} async-done(((bf16[256,1408]{1,0:T(8,128)(2,1)}), bf16[2048,1408]{1,0:T(8,128)(2,1)}) %all-gather.12.cloned.1.call-update) | async-done | bytes 5767184 | tf_op jit(solution)/shard_map/all_gather | solution.py:168
  400.7 8.5 %convolution_convert_fusion.1 = bf16[768,1408]{1,0:T(8,128)(2,1)S(1)} fusion(bf16[768,2048]{1,0:T(8,128)(2,1)} %all-gather.8.cloned.1.call-done, bf16[2048,1408]{1,0:T(8,128)(2,1)} %all-gather.12.cloned.1.call-done), kind=kOutput, calls=%fused_computation.22 | convolution fusion | flops 4430266368 | bytes 11075584 | tf_op jit(solution)/shard_map/dot_general | solution.py:171
  409.2 2.7 collective-permute-start.4
  411.9 2.4 maximum_convert_fusion
  414.3 2.5 maximum_convert_fusion.1
  416.9 77.2 %all-gather.14.cloned.1.call-done = bf16[1408,2048]{1,0:T(8,128)(2,1)} async-done(((bf16[1408,256]{1,0:T(8,128)(2,1)}), bf16[1408,2048]{1,0:T(8,128)(2,1)}) %all-gather.14.cloned.1.call-update) | async-done | bytes 5767184 | tf_op jit(solution)/shard_map/all_gather | solution.py:182
  494.1 17.6 %convolution_convert_fusion = bf16[768,2048]{1,0:T(8,128)(2,1)} fusion(bf16[1408,2048]{1,0:T(8,128)(2,1)} %all-gather.14.cloned.1.call-done, f32[770,1408]{1,0:T(8,128)} %maximum_convert_fusion.1, f32[770,1408]{1,0:T(8,128)} %maximum_convert_fusion, f32[1408]{0:T(1024)S(1)} %get-tuple-element.200, f32[1408]{0:T(1024)S(1)} %get-tuple-element.201, ...), kind=kOutput, calls=%fused_computation.21 | convolution fusion | flops 4448059392 | bytes 34898944 | tf_op jit(solution)/shard_map/dot_general | solution.py:183
  511.8 36.2 %reduce-scatter.5.cloned.1.call-done = bf16[192,2048]{1,0:T(8,128)(2,1)} async-done(((bf16[768,2048]{1,0:T(8,128)(2,1)}), bf16[192,2048]{1,0:T(8,128)(2,1)}) %reduce-scatter.5.cloned.1.call-update) | async-done | bytes 786448 | tf_op jit(solution)/shard_map/reduce_scatter | solution.py:184
  548.0 2.3 fusion.17
  (134 shorter events, 29.4 us)
Async XLA Ops:
  6.5 114.6 %copy-start = (bf16[512,2048]{1,0:T(8,128)(2,1)S(1)}, bf16[512,2048]{1,0:T(8,128)(2,1)}, u32[]{:S(2)}) copy-start(bf16[512,2048]{1,0:T(8,128)(2,1)} %param.36) | copy-start | bytes 6291460
  6.5 100.9 %all-gather.16.cloned.1.call-start = ((), (), s32[]{:S(2)}) async-start(), calls=%async_computation.8 | async-start | bytes 2359296 | tf_op jit(solution)/shard_map/all_gather | solution.py:20
  8.2 19.0 %copy-start.14 = (bf16[4,64]{1,0:T(4,128)(2,1)S(1)}, bf16[4,64]{1,0:T(4,128)(2,1)}, u32[]{:S(2)}) copy-start(bf16[4,64]{1,0:T(4,128)(2,1)} %param.33) | copy-start | bytes 1540
  8.2 22.4 %collective-permute-start = (bf16[3,512]{0,1:T(8,128)(2,1)}, bf16[3,512]{0,1:T(8,128)(2,1)}, u32[]{:S(2)}, u32[]{:S(2)}) collective-permute-start(bf16[3,512]{0,1:T(8,128)(2,1)} %copy.49), channel_id=1, source_target_pairs={{0,4},{4,8},{8,12},{12,16},{16,20},{20,24},{24,28},{1,5},{5,9},{9,... | collective-permute-start | bytes 9224 | tf_op jit(solution)/shard_map/ppermute | solution.py:15
  15.3 13.5 %copy-start.7 = (bf16[768,64]{0,1:T(8,128)(2,1)S(1)}, bf16[768,64]{0,1:T(8,128)(2,1)}, u32[]{:S(2)}) copy-start(bf16[768,64]{0,1:T(8,128)(2,1)} %param.25) | copy-start | bytes 294916
  15.3 13.4 %collective-permute-start.2 = (bf16[3,64]{0,1:T(8,128)(2,1)}, bf16[3,64]{0,1:T(8,128)(2,1)}, u32[]{:S(2)}, u32[]{:S(2)}) collective-permute-start(bf16[3,64]{0,1:T(8,128)(2,1)} %slice.146), channel_id=1, source_target_pairs={{0,4},{4,8},{8,12},{12,16},{16,20},{20,24},{24,28},{1,5},{5,9},{9,... | collective-permute-start | bytes 1160 | tf_op jit(solution)/shard_map/ppermute | solution.py:15
  28.7 3.5 copy-start.12
  28.7 3.5 copy-start.13
  42.0 42.1 %copy-start.15 = (bf16[4,64]{1,0:T(4,128)(2,1)S(1)}, bf16[4,64]{1,0:T(4,128)(2,1)}, u32[]{:S(2)}) copy-start(bf16[4,64]{1,0:T(4,128)(2,1)} %param.34) | copy-start | bytes 1540
  57.6 0.7 copy-start.2
  57.6 30.0 %copy-start.8 = (bf16[768,64]{0,1:T(8,128)(2,1)S(1)}, bf16[768,64]{0,1:T(8,128)(2,1)}, u32[]{:S(2)}) copy-start(bf16[768,64]{0,1:T(8,128)(2,1)} %param.26) | copy-start | bytes 294916
  57.6 30.5 %copy-start.16 = (f32[64]{0:T(128)S(1)}, f32[64]{0:T(128)}, u32[]{:S(2)}) copy-start(f32[64]{0:T(128)} %get-tuple-element.241) | copy-start | bytes 772
  57.6 30.5 %copy-start.17 = (f32[64]{0:T(128)S(1)}, f32[64]{0:T(128)}, u32[]{:S(2)}) copy-start(f32[64]{0:T(128)} %get-tuple-element.242) | copy-start | bytes 772
  57.7 30.5 %copy-start.18 = (f32[64]{0:T(128)S(1)}, f32[64]{0:T(128)}, u32[]{:S(2)}) copy-start(f32[64]{0:T(128)} %get-tuple-element.243) | copy-start | bytes 772
  57.7 30.5 %copy-start.19 = (f32[64]{0:T(128)S(1)}, f32[64]{0:T(128)}, u32[]{:S(2)}) copy-start(f32[64]{0:T(128)} %get-tuple-element.244) | copy-start | bytes 772
  58.4 125.2 %reduce-scatter.3.cloned.1.call-start = ((), (), s32[]{:S(2)}) async-start(), calls=%async_computation.2 | async-start | bytes 7864320 | tf_op jit(solution)/shard_map/reduce_scatter | solution.py:157
  59.2 28.4 %collective-permute-start.1 = (bf16[3,64]{0,1:T(8,128)(2,1)S(1)}, bf16[3,64]{0,1:T(8,128)(2,1)S(1)}, u32[]{:S(2)}, u32[]{:S(2)}) collective-permute-start(bf16[3,64]{0,1:T(8,128)(2,1)S(1)} %slice.137), channel_id=1, source_target_pairs={{0,4},{4,8},{8,12},{12,16},{16,20},{20,24},{24,28},{1,5},{5,9},{9,... | collective-permute-start | bytes 1160 | tf_op jit(solution)/shard_map/ppermute | solution.py:15
  115.1 3.0 copy-start.6
  115.1 3.0 copy-start.21
  119.4 1.1 copy-start.3
  120.3 0.8 copy-start.20
  125.9 59.5 %copy-start.11 = (f32[2048]{0:T(1024)S(1)}, f32[2048]{0:T(1024)}, u32[]{:S(2)}) copy-start(f32[2048]{0:T(1024)} %param.38) | copy-start | bytes 24580
  126.0 152.1 %all-gather.10.cloned.1.call-start = ((), (), s32[]{:S(2)}) async-start(), calls=%async_computation.4 | async-start | bytes 6488064 | tf_op jit(solution)/shard_map/all_gather | solution.py:167
  126.7 179.5 %all-gather.8.cloned.1.call-start = ((), (), s32[]{:S(2)}) async-start(), calls=%async_computation.3 | async-start | bytes 3932160 | tf_op jit(solution)/shard_map/all_gather | solution.py:165
  185.4 2.4 copy-start.9
  185.4 2.4 copy-start.10
  186.6 214.1 %all-gather.12.cloned.1.call-start = ((), (), s32[]{:S(2)}) async-start(), calls=%async_computation.5 | async-start | bytes 6488064 | tf_op jit(solution)/shard_map/all_gather | solution.py:168
  187.2 306.9 %all-gather.14.cloned.1.call-start = ((), (), s32[]{:S(2)}) async-start(), calls=%async_computation.6 | async-start | bytes 6488064 | tf_op jit(solution)/shard_map/all_gather | solution.py:182
  187.8 360.2 %reduce-scatter.5.cloned.1.call-start = ((), (), s32[]{:S(2)}) async-start(), calls=%async_computation.7 | async-start | bytes 3932160 | tf_op jit(solution)/shard_map/reduce_scatter | solution.py:184
  314.5 1.3 copy-start.4
  315.9 96.0 %collective-permute-start.3 = (bf16[2,1408]{1,0:T(2,128)(2,1)S(1)}, bf16[2,1408]{1,0:T(2,128)(2,1)S(1)}, u32[]{:S(2)}, u32[]{:S(2)}) collective-permute-start(bf16[2,1408]{1,0:T(2,128)(2,1)S(1)} %slice.182), channel_id=1, source_target_pairs={{0,4},{4,8},{8,12},{12,16},{16,20},{20,24},{24,28},{1,5},{5,9},{9,... | collective-permute-start | bytes 16904 | tf_op jit(solution)/shard_map/ppermute | solution.py:15
  400.7 11.2 %copy-start.5 = (bf16[768,1408]{1,0:T(8,128)(2,1)S(1)}, bf16[768,1408]{1,0:T(8,128)(2,1)}, u32[]{:S(2)}) copy-start(bf16[768,1408]{1,0:T(8,128)(2,1)} %copy-done.4) | copy-start | bytes 6488068
  409.2 5.1 collective-permute-start.4
  511.8 38.5 %copy-start.1 = (bf16[512,2048]{1,0:T(8,128)(2,1)S(1)}, bf16[512,2048]{1,0:T(8,128)(2,1)}, u32[]{:S(2)}) copy-start(bf16[512,2048]{1,0:T(8,128)(2,1)} %param.36) | copy-start | bytes 6291460
Sparse Core Ops, SparseCore 0:
  58.5 48.9 all-gather.15
  126.1 57.4 reduce-scatter.2
  185.7 92.2 all-gather.9
  279.5 26.6 all-gather.7
  308.2 92.4 all-gather.11
  402.6 91.5 all-gather.13
  511.9 36.0 reduce-scatter.4
where the time goes:
time: 559 us; the launch traced here: 557 us
  waiting for transfers between devices  389 us (70%)
  matrix products  46.6 us (8%)
  other arithmetic  38.4 us (7%)
  local copies, waits for them, and re-layouts  30.2 us (5%)
  blocking collectives  19.2 us (3%)
  starting transfers between devices  18.3 us (3%)
  between operations  14.6 us (3%)
    all_gather x1, waiting for transfers between devices, on_device(): lax.all_gather(feedforward_gate_weight, 'sp', axis=0, tiled=True)  90.1 us
    all_gather x1, waiting for transfers between devices, on_device(): lax.all_gather(feedforward_value_weight, 'sp', axis=0, tiled=True)  81.4 us
    all_gather x1, waiting for transfers between devices, on_device(): lax.all_gather(feedforward_down_weight, 'sp', axis=1, tiled=True)  77.2 us
    reduce_scatter x1, waiting for transfers between devices, on_device(): lax.psum_scatter(jnp.dot(normed, mixer_output_weight, preferred_element_t...  56.8 us
    reduce_scatter x1, waiting for transfers between devices, on_device(): lax.psum_scatter(partial_down.astype(jnp.bfloat16), 'tp', scatter_dimensi...  36.2 us
    all_gather x1, waiting for transfers between devices, on_device(): lax.all_gather(channel_norm(stream, feedforward_norm_gain), 'tp', axis=0,...  28.1 us
    unnamed x1, blocking collectives  19.2 us
    ppermute x5, starting transfers between devices, from_behind(): return lax.ppermute(value, axis, pairs)  18.1 us
  transfers between devices with their start and end apart: 12, of which 7 were waited for; matrix products, arithmetic and copies ran while one was open for 8% of the time, Pallas kernels for 0%

commit v1 on v0

--- a/solution.py
+++ b/solution.py
@@ -179,7 +179,14 @@
         jax.nn.silu(causal_taps(gate_rows, rim_gate, gate_filter_taps))
         * causal_taps(value_rows, rim_value, single_value_filter_taps)
     ).astype(jnp.bfloat16)
-    down_full = lax.all_gather(feedforward_down_weight, "sp", axis=1, tiled=True)
+    size = lax.axis_size("sp")
+    route = [(i_2, (i_2 + 1) % size) for i_2 in range(size)]
+    parts = [feedforward_down_weight]
+    for reach in range(1, size):
+        parts = [lax.ppermute(parts[0], "sp", route), *parts]
+    full = jnp.concatenate(parts, axis=1)
+    offset_2 = (lax.axis_index("sp") + 1) * parts[-1].shape[1]
+    down_full = jnp.roll(full, offset_2, axis=1)
     partial_down = jnp.dot(hidden, down_full, preferred_element_type=jnp.float32)
     down = lax.psum_scatter(
         partial_down.astype(jnp.bfloat16), "tp", scatter_dimension=0, tiled=True

time: 559 us -> 540 us (0.966)
  waiting for transfers between devices: 389 us -> 351 us
  local copies, waits for them, and re-layouts: 30.2 us -> 53.1 us
    ppermute x0 -> x7, waiting for transfers between devices: none -> 199 us  [on_device(): parts = [lax.ppermute(parts[0], 'sp', route), *parts]]
    all_gather x1, waiting for transfers between devices: 81.4 us -> 0.01 us  [on_device(): lax.all_gather(feedforward_value_weight, 'sp', axis=0, tiled=True)]
    all_gather x1 -> x0, waiting for transfers between devices: 77.2 us -> none  [on_device(): lax.all_gather(feedforward_down_weight, 'sp', axis=1, tiled=True)]
    all_gather x1, waiting for transfers between devices: 90.1 us -> 38.1 us  [on_device(): lax.all_gather(feedforward_gate_weight, 'sp', axis=0, tiled=True)]
    all_gather x1, waiting for transfers between devices: 28.1 us -> 0.01 us  [on_device(): lax.all_gather(channel_norm(stream, feedforward_norm_gain), 'tp', axis=0,...]
    unnamed x50 -> x75, local copies, waits for them, and re-layouts: 8.84 us -> 31.1 us
  transfers between devices with their start and end apart: 12 -> 18, of which waited for: 7 -> 12; matrix products, arithmetic and copies ran while one was open for 8% -> 12% of each run, Pallas kernels for 0% -> 0%
where the time goes in v1:
time: 540 us; the launch traced here: 538 us
  waiting for transfers between devices  351 us (65%)
  local copies, waits for them, and re-layouts  53.1 us (10%)
  matrix products  43.8 us (8%)
  other arithmetic  38.6 us (7%)
  blocking collectives  19.2 us (4%)
  starting transfers between devices  17.5 us (3%)
  between operations  14.7 us (3%)
    ppermute x7, waiting for transfers between devices, on_device(): parts = [lax.ppermute(parts[0], 'sp', route), *parts]  199 us
    reduce_scatter x1, waiting for transfers between devices, on_device(): lax.psum_scatter(jnp.dot(normed, mixer_output_weight, preferred_element_t...  56.7 us
    reduce_scatter x1, waiting for transfers between devices, on_device(): lax.psum_scatter(partial_down.astype(jnp.bfloat16), 'tp', scatter_dimensi...  38.8 us
    all_gather x1, waiting for transfers between devices, on_device(): lax.all_gather(feedforward_gate_weight, 'sp', axis=0, tiled=True)  38.1 us
    unnamed x75, local copies, waits for them, and re-layouts  31.1 us
    unnamed x1, blocking collectives  19.2 us
    all_gather x1, waiting for transfers between devices, entering_2(): pieces = jax.tree.map(lambda part: lax.all_gather(part, axis), value)  16.8 us
    ppermute x5, starting transfers between devices, from_behind(): return lax.ppermute(value, axis, pairs)  15.8 us
  transfers between devices with their start and end apart: 18, of which 12 were waited for; matrix products, arithmetic and copies ran while one was open for 12% of the time, Pallas kernels for 0%

profile of v1, /device:TPU:0, one launch (start us, length us, event | category | flops | bytes accessed | tf_op | source)
XLA Modules:
  0.0 538.0 jit_solution(17772516242664140963)
XLA Ops:
  7.6 4.9 collective-permute-start
  13.3 3.4 collective-permute-start.2
  19.2 1.4 reduce_window_sum.22
  20.6 1.1 slice_reduce_fusion
  22.7 1.4 slice_convert_fusion.3
  24.1 1.4 bitcast_convert_fusion.3
  25.6 2.3 copy.50
  27.8 1.2 copy.58
  30.3 1.6 maximum_convert_fusion.2
  31.8 3.4 fusion.44
  35.2 2.6 reshape.164
  37.9 2.9 multiply_convert_fusion.1
  40.8 1.5 convolution_bitcast_fusion
  42.3 15.6 %while.27 = (s32[]{:T(128)}, f32[1,8,64,64]{3,2,1,0:T(8,128)S(1)}, f32[6,1,8,64,64]{4,3,2,1,0:T(8,128)}, f32[6,1,8]{2,1,0:T(1,128)}, f32[6,1,8,64,64]{3,4,2,0,1:T(8,128)}, /*index=5*/s32[]{:T(128)}, s32[]{:T(128)}) while((s32[]{:T(128)}, f32[1,8,64,64]{3,2,1,0:T(8,128)S(1)}, f32[6,1,8,64,64]{4,3,2,1,0:T(8,128)}, ...), condition=%wide.region_2.3_spmd.clone, body=%wide.region_1.2_spmd.clone.sunk | while | flops 131075 | bytes 1310924 | solution.py:130
  59.5 3.4 collective-permute-start.1
  63.1 2.3 copy.68
  67.5 19.2 %all-reduce = f32[64]{0:T(128)S(1)} all-reduce(f32[64]{0:T(128)S(1)} %exponential_dynamic-update-slice_fusion), channel_id=2, replica_groups=mesh['sp'=8,'tp'=4] {'sp'}, use_global_device_ids=true, to_apply=%add | all-reduce | flops 64 | bytes 512
  89.4 2.1 fusion.51
  91.5 16.8 %all-gather.13.cloned.1.call-done = f32[8,8,64,64]{3,2,1,0:T(8,128)} async-done(((f32[1,8,64,64]{3,2,1,0:T(8,128)}), f32[8,8,64,64]{3,2,1,0:T(8,128)}) %all-gather.13.cloned.1.call-update) | async-done | bytes 1048592 | tf_op jit(solution)/shard_map/all_gather | solution.py:20
  108.3 7.7 %while.28 = (s32[]{:T(128)}, f32[1,8,64,64]{3,2,1,0:T(8,128)S(1)}, s32[]{:T(128)}, f32[8,1,8]{2,1,0:T(1,128)S(1)}, f32[8,1,8,64,64]{4,3,2,1,0:T(8,128)}, /*index=5*/s32[]{:T(128)}, s32[]{:T(128)}) while((s32[]{:T(128)}, f32[1,8,64,64]{3,2,1,0:T(8,128)S(1)}, s32[]{:T(128)}, f32[8,1,8]{2,1,0:T(1,128)S(1)}, ...), condition=%wide.region_5.6_spmd.clone, body=%wide.region_4.5_spmd.clone.sunk | while | flops 131076 | bytes 393425 | solution.py:29
  116.0 3.0 fusion.28
  119.0 1.3 fusion.27
  122.0 4.8 fusion.37
  127.6 56.7 %reduce-scatter.3.cloned.1.call-done = f32[192,2048]{1,0:T(8,128)} async-done(((f32[768,2048]{1,0:T(8,128)}), f32[192,2048]{1,0:T(8,128)}) %reduce-scatter.3.cloned.1.call-update) | async-done | bytes 1572880 | tf_op jit(solution)/shard_map/reduce_scatter | solution.py:157
  184.4 1.9 fusion.19
  186.3 1.1 fusion.21
  187.5 1.5 collective-permute-start.5
  189.1 27.6 %collective-permute-done.5 = bf16[1408,256]{1,0:T(8,128)(2,1)S(1)} collective-permute-done((bf16[1408,256]{1,0:T(8,128)(2,1)S(1)}, bf16[1408,256]{1,0:T(8,128)(2,1)S(1)}, u32[]{:S(2)}, u32[]{:S(2)}) %collective-permute-start.5) | collective-permute-done | bytes 720928 | tf_op jit(solution)/shard_map/ppermute | solution.py:186
  216.7 30.0 %collective-permute-done.6 = bf16[1408,256]{1,0:T(8,128)(2,1)S(1)} collective-permute-done((bf16[1408,256]{1,0:T(8,128)(2,1)S(1)}, bf16[1408,256]{1,0:T(8,128)(2,1)S(1)}, u32[]{:S(2)}, u32[]{:S(2)}) %collective-permute-start.6) | collective-permute-done | bytes 720928 | tf_op jit(solution)/shard_map/ppermute | solution.py:186
  247.6 36.3 %collective-permute-done.7 = bf16[1408,256]{1,0:T(8,128)(2,1)S(1)} collective-permute-done((bf16[1408,256]{1,0:T(8,128)(2,1)S(1)}, bf16[1408,256]{1,0:T(8,128)(2,1)S(1)}, u32[]{:S(2)}, u32[]{:S(2)}) %collective-permute-start.7) | collective-permute-done | bytes 720928 | tf_op jit(solution)/shard_map/ppermute | solution.py:186
  284.8 36.1 %collective-permute-done.8 = bf16[1408,256]{1,0:T(8,128)(2,1)S(1)} collective-permute-done((bf16[1408,256]{1,0:T(8,128)(2,1)S(1)}, bf16[1408,256]{1,0:T(8,128)(2,1)S(1)}, u32[]{:S(2)}, u32[]{:S(2)}) %collective-permute-start.8) | collective-permute-done | bytes 720928 | tf_op jit(solution)/shard_map/ppermute | solution.py:186
  321.8 21.2 %collective-permute-done.9 = bf16[1408,256]{1,0:T(8,128)(2,1)S(1)} collective-permute-done((bf16[1408,256]{1,0:T(8,128)(2,1)S(1)}, bf16[1408,256]{1,0:T(8,128)(2,1)S(1)}, u32[]{:S(2)}, u32[]{:S(2)}) %collective-permute-start.9) | collective-permute-done | bytes 720928 | tf_op jit(solution)/shard_map/ppermute | solution.py:186
  343.9 19.7 %collective-permute-done.10 = bf16[1408,256]{1,0:T(8,128)(2,1)} collective-permute-done((bf16[1408,256]{1,0:T(8,128)(2,1)S(1)}, bf16[1408,256]{1,0:T(8,128)(2,1)}, u32[]{:S(2)}, u32[]{:S(2)}) %collective-permute-start.10) | collective-permute-done | bytes 720928 | tf_op jit(solution)/shard_map/ppermute | solution.py:186
  363.7 27.7 %collective-permute-done.11 = bf16[1408,256]{1,0:T(8,128)(2,1)} collective-permute-done((bf16[1408,256]{1,0:T(8,128)(2,1)}, bf16[1408,256]{1,0:T(8,128)(2,1)}, u32[]{:S(2)}, u32[]{:S(2)}) %collective-permute-start.11) | collective-permute-done | bytes 720928 | tf_op jit(solution)/shard_map/ppermute | solution.py:186
  391.4 2.1 constant_dynamic-update-slice_fusion.15
  393.5 2.2 constant_dynamic-update-slice_fusion.14
  401.6 2.1 constant_dynamic-update-slice_fusion.7
  403.7 2.1 constant_dynamic-update-slice_fusion.6
  411.6 8.3 %convolution_convert_fusion = bf16[768,1408]{1,0:T(8,128)(2,1)S(1)} fusion(bf16[768,2048]{1,0:T(8,128)(2,1)} %all-gather.7.cloned.1.call-done, bf16[2048,1408]{1,0:T(8,128)(2,1)} %all-gather.11.cloned.1.call-done), kind=kOutput, calls=%fused_computation.24 | convolution fusion | flops 4430266368 | bytes 11075584 | tf_op jit(solution)/shard_map/dot_general | solution.py:171
  419.9 1.4 copy-done.13
  421.4 1.5 collective-permute-start.4
  422.9 38.1 %all-gather.9.cloned.1.call-done = bf16[2048,1408]{1,0:T(8,128)(2,1)} async-done(((bf16[256,1408]{1,0:T(8,128)(2,1)}), bf16[2048,1408]{1,0:T(8,128)(2,1)}) %all-gather.9.cloned.1.call-update) | async-done | bytes 5767184 | tf_op jit(solution)/shard_map/all_gather | solution.py:167
  461.0 8.5 %convolution_convert_fusion.1 = bf16[768,1408]{1,0:T(8,128)(2,1)S(1)} fusion(bf16[768,2048]{1,0:T(8,128)(2,1)} %all-gather.7.cloned.1.call-done, bf16[2048,1408]{1,0:T(8,128)(2,1)} %all-gather.9.cloned.1.call-done), kind=kOutput, calls=%fused_computation.25 | convolution fusion | flops 4430266368 | bytes 11075584 | tf_op jit(solution)/shard_map/dot_general | solution.py:170
  469.5 2.5 collective-permute-start.3
  473.4 2.4 maximum_convert_fusion
  475.8 14.3 %fusion.11 = bf16[768,2048]{1,0:T(8,128)(2,1)} fusion(bf16[1408,4096]{1,0:T(8,128)(2,1)} %constant_dynamic-update-slice_fusion, s32[]{:T(128)S(6)} %select_n.54, f32[770,1408]{1,0:T(8,128)S(1)} %maximum_convert_fusion.1, f32[770,1408]{1,0:T(8,128)} %maximum_convert_fusion, f32[1408]{0:T(1024)S(1)} %get-tuple-element.200, f32[1408]{0:T(1024)S(1)} %get-tuple-element.201, ...), kind=kOutput, calls=%fused_computation.23 | convolution fusion | flops 4448059392 | bytes 34914308 | tf_op jit(solution)/shard_map/dot_general | solution.py:190
  490.1 38.8 %reduce-scatter.5.cloned.1.call-done = bf16[192,2048]{1,0:T(8,128)(2,1)} async-done(((bf16[768,2048]{1,0:T(8,128)(2,1)}), bf16[192,2048]{1,0:T(8,128)(2,1)}) %reduce-scatter.5.cloned.1.call-update) | async-done | bytes 786448 | tf_op jit(solution)/shard_map/reduce_scatter | solution.py:191
  528.9 2.3 fusion.22
  (171 shorter events, 54.4 us)
Async XLA Ops:
  6.5 115.4 %copy-start = (bf16[512,2048]{1,0:T(8,128)(2,1)S(1)}, bf16[512,2048]{1,0:T(8,128)(2,1)}, u32[]{:S(2)}) copy-start(bf16[512,2048]{1,0:T(8,128)(2,1)} %param.36) | copy-start | bytes 6291460
  6.5 22.5 %copy-start.16 = (bf16[768,64]{0,1:T(8,128)(2,1)S(1)}, bf16[768,64]{0,1:T(8,128)(2,1)}, u32[]{:S(2)}) copy-start(bf16[768,64]{0,1:T(8,128)(2,1)} %param.25) | copy-start | bytes 294916
  6.5 101.8 %all-gather.13.cloned.1.call-start = ((), (), s32[]{:S(2)}) async-start(), calls=%async_computation.7 | async-start | bytes 2359296 | tf_op jit(solution)/shard_map/all_gather | solution.py:20
  7.6 22.7 %collective-permute-start = (bf16[3,512]{0,1:T(8,128)(2,1)S(1)}, bf16[3,512]{0,1:T(8,128)(2,1)S(1)}, u32[]{:S(2)}, u32[]{:S(2)}) collective-permute-start(bf16[3,512]{0,1:T(8,128)(2,1)S(1)} %copy.49), channel_id=1, source_target_pairs={{0,4},{4,8},{8,12},{12,16},{16,20},{20,24},{24,28},{1,5},{5,9},{9,... | collective-permute-start | bytes 9224 | tf_op jit(solution)/shard_map/ppermute | solution.py:15
  13.3 15.7 %collective-permute-start.2 = (bf16[3,64]{0,1:T(8,128)(2,1)S(1)}, bf16[3,64]{0,1:T(8,128)(2,1)S(1)}, u32[]{:S(2)}, u32[]{:S(2)}) collective-permute-start(bf16[3,64]{0,1:T(8,128)(2,1)S(1)} %slice.146), channel_id=1, source_target_pairs={{0,4},{4,8},{8,12},{12,16},{16,20},{20,24},{24,28},{1,5},{5,9},{9,... | collective-permute-start | bytes 1160 | tf_op jit(solution)/shard_map/ppermute | solution.py:15
  42.3 23.1 %copy-start.25 = (u32[32]{0:T(128)S(1)}, u32[32]{0:T(128)}, u32[]{:S(2)}) copy-start(u32[32]{0:T(128)} %constant.110) | copy-start | bytes 388
  42.3 25.2 %copy-start.20 = (bf16[4,64]{1,0:T(4,128)(2,1)S(1)}, bf16[4,64]{1,0:T(4,128)(2,1)}, u32[]{:S(2)}) copy-start(bf16[4,64]{1,0:T(4,128)(2,1)} %param.34) | copy-start | bytes 1540
  57.9 0.7 copy-start.2
  57.9 31.4 %copy-start.21 = (f32[64]{0:T(128)S(1)}, f32[64]{0:T(128)}, u32[]{:S(2)}) copy-start(f32[64]{0:T(128)} %get-tuple-element.241) | copy-start | bytes 772
  57.9 31.4 %copy-start.22 = (f32[64]{0:T(128)S(1)}, f32[64]{0:T(128)}, u32[]{:S(2)}) copy-start(f32[64]{0:T(128)} %get-tuple-element.242) | copy-start | bytes 772
  57.9 31.4 %copy-start.23 = (f32[64]{0:T(128)S(1)}, f32[64]{0:T(128)}, u32[]{:S(2)}) copy-start(f32[64]{0:T(128)} %get-tuple-element.243) | copy-start | bytes 772
  58.7 125.7 %reduce-scatter.3.cloned.1.call-start = ((), (), s32[]{:S(2)}) async-start(), calls=%async_computation.2 | async-start | bytes 7864320 | tf_op jit(solution)/shard_map/reduce_scatter | solution.py:157
  59.5 28.4 %collective-permute-start.1 = (bf16[3,64]{0,1:T(8,128)(2,1)S(1)}, bf16[3,64]{0,1:T(8,128)(2,1)S(1)}, u32[]{:S(2)}, u32[]{:S(2)}) collective-permute-start(bf16[3,64]{0,1:T(8,128)(2,1)S(1)} %slice.137), channel_id=1, source_target_pairs={{0,4},{4,8},{8,12},{12,16},{16,20},{20,24},{24,28},{1,5},{5,9},{9,... | collective-permute-start | bytes 1160 | tf_op jit(solution)/shard_map/ppermute | solution.py:15
  108.3 10.7 %copy-start.26 = (f32[6,128,128]{2,1,0:T(8,128)S(1)}, f32[6,128,128]{2,1,0:T(8,128)}, u32[]{:S(2)}) copy-start(f32[6,128,128]{2,1,0:T(8,128)} %fusion.51) | copy-start | bytes 1179652
  116.0 3.0 copy-start.15
  120.3 1.1 copy-start.3
  120.3 1.7 copy-start.24
  126.8 59.5 %copy-start.19 = (f32[2048]{0:T(1024)S(1)}, f32[2048]{0:T(1024)}, u32[]{:S(2)}) copy-start(f32[2048]{0:T(1024)} %param.38) | copy-start | bytes 24580
  126.8 60.7 %copy-start.4 = (bf16[1408,256]{1,0:T(8,128)(2,1)S(1)}, bf16[1408,256]{1,0:T(8,128)(2,1)}, u32[]{:S(2)}) copy-start(bf16[1408,256]{1,0:T(8,128)(2,1)} %param.43) | copy-start | bytes 2162692
  126.8 284.8 %all-gather.11.cloned.1.call-start = ((), (), s32[]{:S(2)}) async-start(), calls=%async_computation.5 | async-start | bytes 6488064 | tf_op jit(solution)/shard_map/all_gather | solution.py:168
  127.6 236.0 %copy-start.17 = (bf16[3,1408]{1,0:T(4,128)(2,1)S(1)}, bf16[3,1408]{1,0:T(4,128)(2,1)}, u32[]{:S(2)}) copy-start(bf16[3,1408]{1,0:T(4,128)(2,1)} %param.42) | copy-start | bytes 25348
  127.6 236.0 %copy-start.18 = (bf16[3,1408]{1,0:T(4,128)(2,1)S(1)}, bf16[3,1408]{1,0:T(4,128)(2,1)}, u32[]{:S(2)}) copy-start(bf16[3,1408]{1,0:T(4,128)(2,1)} %param.41) | copy-start | bytes 25348
  127.6 284.0 %all-gather.7.cloned.1.call-start = ((), (), s32[]{:S(2)}) async-start(), calls=%async_computation.3 | async-start | bytes 3932160 | tf_op jit(solution)/shard_map/all_gather | solution.py:165
  187.5 273.5 %all-gather.9.cloned.1.call-start = ((), (), s32[]{:S(2)}) async-start(), calls=%async_computation.4 | async-start | bytes 6488064 | tf_op jit(solution)/shard_map/all_gather | solution.py:167
  187.5 29.2 %collective-permute-start.5 = (bf16[1408,256]{1,0:T(8,128)(2,1)S(1)}, bf16[1408,256]{1,0:T(8,128)(2,1)S(1)}, u32[]{:S(2)}, u32[]{:S(2)}) collective-permute-start(bf16[1408,256]{1,0:T(8,128)(2,1)S(1)} %copy-done.4), channel_id=1, source_target_pairs={{0,4},{4,8},{8,12},{12,16},{16,20},{20,24},{24,28},{28,0},{1,5},{5... | collective-permute-start | bytes 2162696 | tf_op jit(solution)/shard_map/ppermute | solution.py:186
  189.0 339.8 %reduce-scatter.5.cloned.1.call-start = ((), (), s32[]{:S(2)}) async-start(), calls=%async_computation.6 | async-start | bytes 3932160 | tf_op jit(solution)/shard_map/reduce_scatter | solution.py:191
  216.7 30.0 %collective-permute-start.6 = (bf16[1408,256]{1,0:T(8,128)(2,1)S(1)}, bf16[1408,256]{1,0:T(8,128)(2,1)S(1)}, u32[]{:S(2)}, u32[]{:S(2)}) collective-permute-start(bf16[1408,256]{1,0:T(8,128)(2,1)S(1)} %collective-permute-done.5), channel_id=1, source_target_pairs={{0,4},{4,8},{8,12},{12,16},{16,20},{20,24},{24,28},{28,0},{1,5},{5... | collective-permute-start | bytes 2162696 | tf_op jit(solution)/shard_map/ppermute | solution.py:186
  246.7 0.9 copy-start.5
  247.6 36.3 %collective-permute-start.7 = (bf16[1408,256]{1,0:T(8,128)(2,1)S(1)}, bf16[1408,256]{1,0:T(8,128)(2,1)S(1)}, u32[]{:S(2)}, u32[]{:S(2)}) collective-permute-start(bf16[1408,256]{1,0:T(8,128)(2,1)S(1)} %collective-permute-done.6), channel_id=1, source_target_pairs={{0,4},{4,8},{8,12},{12,16},{16,20},{20,24},{24,28},{28,0},{1,5},{5... | collective-permute-start | bytes 2162696 | tf_op jit(solution)/shard_map/ppermute | solution.py:186
  283.9 0.9 copy-start.7
  284.8 36.1 %collective-permute-start.8 = (bf16[1408,256]{1,0:T(8,128)(2,1)S(1)}, bf16[1408,256]{1,0:T(8,128)(2,1)S(1)}, u32[]{:S(2)}, u32[]{:S(2)}) collective-permute-start(bf16[1408,256]{1,0:T(8,128)(2,1)S(1)} %collective-permute-done.7), channel_id=1, source_target_pairs={{0,4},{4,8},{8,12},{12,16},{16,20},{20,24},{24,28},{28,0},{1,5},{5... | collective-permute-start | bytes 2162696 | tf_op jit(solution)/shard_map/ppermute | solution.py:186
  320.9 0.9 copy-start.9
  321.8 21.2 %collective-permute-start.9 = (bf16[1408,256]{1,0:T(8,128)(2,1)S(1)}, bf16[1408,256]{1,0:T(8,128)(2,1)S(1)}, u32[]{:S(2)}, u32[]{:S(2)}) collective-permute-start(bf16[1408,256]{1,0:T(8,128)(2,1)S(1)} %collective-permute-done.8), channel_id=1, source_target_pairs={{0,4},{4,8},{8,12},{12,16},{16,20},{20,24},{24,28},{28,0},{1,5},{5... | collective-permute-start | bytes 2162696 | tf_op jit(solution)/shard_map/ppermute | solution.py:186
  343.0 0.9 copy-start.11
  343.9 19.7 %collective-permute-start.10 = (bf16[1408,256]{1,0:T(8,128)(2,1)S(1)}, bf16[1408,256]{1,0:T(8,128)(2,1)}, u32[]{:S(2)}, u32[]{:S(2)}) collective-permute-start(bf16[1408,256]{1,0:T(8,128)(2,1)S(1)} %collective-permute-done.9), channel_id=1, source_target_pairs={{0,4},{4,8},{8,12},{12,16},{16,20},{20,24},{24,28},{28,0},{1,5},{5... | collective-permute-start | bytes 2162696 | tf_op jit(solution)/shard_map/ppermute | solution.py:186
  363.6 27.9 %collective-permute-start.11 = (bf16[1408,256]{1,0:T(8,128)(2,1)}, bf16[1408,256]{1,0:T(8,128)(2,1)}, u32[]{:S(2)}, u32[]{:S(2)}) collective-permute-start(bf16[1408,256]{1,0:T(8,128)(2,1)} %collective-permute-done.10), channel_id=1, source_target_pairs={{0,4},{4,8},{8,12},{12,16},{16,20},{20,24},{24,28},{28,0},{1,5},{5... | collective-permute-start | bytes 2162696 | tf_op jit(solution)/shard_map/ppermute | solution.py:186
  363.6 32.1 %copy-start.12 = (bf16[1408,256]{1,0:T(8,128)(2,1)S(1)}, bf16[1408,256]{1,0:T(8,128)(2,1)}, u32[]{:S(2)}) copy-start(bf16[1408,256]{1,0:T(8,128)(2,1)} %copy-done.11) | copy-start | bytes 2162692
  363.6 33.1 %copy-start.10 = (bf16[1408,256]{1,0:T(8,128)(2,1)S(1)}, bf16[1408,256]{1,0:T(8,128)(2,1)}, u32[]{:S(2)}) copy-start(bf16[1408,256]{1,0:T(8,128)(2,1)} %copy-done.9) | copy-start | bytes 2162692
  363.6 34.0 %copy-start.8 = (bf16[1408,256]{1,0:T(8,128)(2,1)S(1)}, bf16[1408,256]{1,0:T(8,128)(2,1)}, u32[]{:S(2)}) copy-start(bf16[1408,256]{1,0:T(8,128)(2,1)} %copy-done.7) | copy-start | bytes 2162692
  393.5 5.1 copy-start.6
  419.9 1.4 copy-start.13
  421.4 50.7 %collective-permute-start.4 = (bf16[2,1408]{1,0:T(2,128)(2,1)S(1)}, bf16[2,1408]{1,0:T(2,128)(2,1)S(1)}, u32[]{:S(2)}, u32[]{:S(2)}) collective-permute-start(bf16[2,1408]{1,0:T(2,128)(2,1)S(1)} %slice.186), channel_id=1, source_target_pairs={{0,4},{4,8},{8,12},{12,16},{16,20},{20,24},{24,28},{1,5},{5,9},{9,... | collective-permute-start | bytes 16904 | tf_op jit(solution)/shard_map/ppermute | solution.py:15
  461.0 11.0 %copy-start.14 = (bf16[768,1408]{1,0:T(8,128)(2,1)S(1)}, bf16[768,1408]{1,0:T(8,128)(2,1)}, u32[]{:S(2)}) copy-start(bf16[768,1408]{1,0:T(8,128)(2,1)} %copy-done.13) | copy-start | bytes 6488068
  469.5 3.9 collective-permute-start.3
  475.8 55.4 %copy-start.1 = (bf16[512,2048]{1,0:T(8,128)(2,1)S(1)}, bf16[512,2048]{1,0:T(8,128)(2,1)}, u32[]{:S(2)}) copy-start(bf16[512,2048]{1,0:T(8,128)(2,1)} %param.36) | copy-start | bytes 6291460
Sparse Core Ops, SparseCore 0:
  58.8 49.4 all-gather.12
  126.9 57.4 reduce-scatter.2
  186.6 133.7 all-gather.10
  321.8 38.7 all-gather.6
  362.6 98.2 all-gather.8
  490.2 38.6 reduce-scatter.4
